TPU v7x, 32 devices: a whole 2x2x4 slice. The times are simulated.
32 devices in a mesh: fs: 4 (over z), rep: 4 (over y, x), tp: 2 (over core).
Axes of the slice: x: 2, y: 2, z: 4, core: 2. Of those that a mesh axis runs over, the one named last changes fastest.
Arguments:
- normed_in: bfloat16 [24576, 2048], P(('fs', 'rep')), may hold values from -6 to 6
- cotan_rec: bfloat16 [24576, 2048], P(('fs', 'rep'), 'tp'), may hold values from -0.0390625 to 0.0390625
- cotan_gate: bfloat16 [24576, 2048], P(('fs', 'rep'), 'tp'), may hold values from -0.0390625 to 0.0390625
- factor_rec: bfloat16 [2048, 512], P('fs'), may hold values from -0.125 to 0.125
- factor_gate: bfloat16 [2048, 512], P('fs'), may hold values from -0.125 to 0.125
- first_rec: float32 [512, 2048], P('fs', 'tp'), may hold values from -6 to 6
- first_gate: float32 [512, 2048], P('fs', 'tp'), may hold values from -6 to 6
- second_rec: float32 [512, 2048], P('fs', 'tp'), may hold values from 0.25 to 4
- second_gate: float32 [512, 2048], P('fs', 'tp'), may hold values from 0.25 to 4
- master_rec: float32 [2048, 2048], P('fs', 'tp'), may hold values from -0.125 to 0.125
- master_gate: float32 [2048, 2048], P('fs', 'tp'), may hold values from -0.125 to 0.125
Outputs:
- update_rec: float32 [2048, 2048], P('fs', 'tp')
- update_gate: float32 [2048, 2048], P('fs', 'tp')
- new_first_rec: float32 [512, 2048], P('fs', 'tp')
- new_first_gate: float32 [512, 2048], P('fs', 'tp')
- new_second_rec: float32 [512, 2048], P('fs', 'tp')
- new_second_gate: float32 [512, 2048], P('fs', 'tp')
- copy_rec: bfloat16 [2048, 2048], P(None, 'tp')
- copy_gate: bfloat16 [2048, 2048], P(None, 'tp')
All inputs are finite; a program needn't handle non-finite values.
Results may differ from a plain program's by a relative error of at most 0.007.
Values may be sent and summed in bfloat16 or wider, within the bound.
A program may use at most 128 MiB of HBM per device.

v0:
```python
import jax
import jax.numpy as jnp
from jax import lax
from jax.sharding import PartitionSpec as P

DR = 2048
RANK = 512


beta_first = 0.8
beta_second = 0.9
scale_floor = 0.25
step_rate = 0.01


def split_product(projected, cotan):
    upper = projected.astype(jnp.bfloat16)
    lower = (projected - upper.astype(jnp.float32)).astype(jnp.bfloat16)
    dims = (((0,), (0,)), ((), ()))
    return lax.dot_general(
        upper, cotan, dims, preferred_element_type=jnp.float32
    ) + lax.dot_general(lower, cotan, dims, preferred_element_type=jnp.float32)


def moments(low, first, second):
    new_first = beta_first * first + (1.0 - beta_first) * low
    new_second = beta_second * second + (1.0 - beta_second) * low * low
    return (new_first, new_second, new_first / jnp.sqrt(new_second))


def body(
    normed_in,
    cotan_rec,
    cotan_gate,
    factor_rec,
    factor_gate,
    first_rec,
    first_gate,
    second_rec,
    second_gate,
    master_rec,
    master_gate,
):
    wide_rec = factor_rec.astype(jnp.float32)
    wide_gate = factor_gate.astype(jnp.float32)
    pieces = (
        lax.all_gather(factor_rec, "fs", axis=0, tiled=True),
        lax.all_gather(factor_gate, "fs", axis=0, tiled=True),
    )
    proj_rec = jnp.dot(normed_in, pieces[0], preferred_element_type=jnp.float32)
    proj_gate = jnp.dot(normed_in, pieces[1], preferred_element_type=jnp.float32)
    part_rec = split_product(proj_rec, cotan_rec)
    part_gate = split_product(proj_gate, cotan_gate)
    low_rec, low_gate = (
        lax.psum_scatter(
            part_rec.astype(jnp.bfloat16), "fs", scatter_dimension=0, tiled=True
        ).astype(jnp.float32),
        lax.psum_scatter(
            part_gate.astype(jnp.bfloat16), "fs", scatter_dimension=0, tiled=True
        ).astype(jnp.float32),
    )
    low_rec, low_gate = (
        lax.psum(low_rec.astype(jnp.bfloat16), "rep").astype(jnp.float32),
        lax.psum(low_gate.astype(jnp.bfloat16), "rep").astype(jnp.float32),
    )
    first_r, second_r, direc_rec = moments(low_rec, first_rec, second_rec)
    first_g, second_g, direc_gate = moments(low_gate, first_gate, second_gate)
    total_rec, total_gate = lax.psum(
        (jnp.sum(direc_rec * direc_rec), jnp.sum(direc_gate * direc_gate)), ("fs", "tp")
    )
    entries = float(RANK * DR)
    scale_rec = 1.0 / jnp.sqrt(total_rec / entries + scale_floor)
    scale_gate = 1.0 / jnp.sqrt(total_gate / entries + scale_floor)
    pieces = (
        lax.all_gather(direc_rec, "fs", axis=0, tiled=True),
        lax.all_gather(direc_gate, "fs", axis=0, tiled=True),
    )
    upd_rec = jnp.dot(wide_rec, pieces[0], precision=lax.Precision.HIGHEST)
    upd_gate = jnp.dot(wide_gate, pieces[1], precision=lax.Precision.HIGHEST)
    upd_rec = upd_rec * scale_rec
    upd_gate = upd_gate * scale_gate
    copy_rec = (master_rec - step_rate * upd_rec).astype(jnp.bfloat16)
    copy_gate = (master_gate - step_rate * upd_gate).astype(jnp.bfloat16)
    whole_rec, whole_gate = (
        lax.all_gather(copy_rec, "fs", axis=0, tiled=True),
        lax.all_gather(copy_gate, "fs", axis=0, tiled=True),
    )
    return (upd_rec, upd_gate, first_r, first_g, second_r, second_g, whole_rec, whole_gate)


def solution(mesh):
    return jax.shard_map(
        body,
        mesh=mesh,
        in_specs=(
            P(("fs", "rep"), None),
            P(("fs", "rep"), "tp"),
            P(("fs", "rep"), "tp"),
            P("fs", None),
            P("fs", None),
            P("fs", "tp"),
            P("fs", "tp"),
            P("fs", "tp"),
            P("fs", "tp"),
            P("fs", "tp"),
            P("fs", "tp"),
        ),
        out_specs=(
            P("fs", "tp"),
            P("fs", "tp"),
            P("fs", "tp"),
            P("fs", "tp"),
            P("fs", "tp"),
            P("fs", "tp"),
            P(None, "tp"),
            P(None, "tp"),
        ),
        check_vma=False,
    )
```

profile of v0, /device:TPU:0, one launch (start us, length us, event | category | flops | bytes accessed | tf_op | source)
XLA Modules:
  0.0 479.8 jit_solution(12746524796464819024)
XLA Ops:
  7.2 0.7 all-gather.7.cloned.1.call-update
  8.0 0.7 all-gather.11.cloned.1.call-update
  8.7 49.3 %all-gather.7.cloned.1.call-done = bf16[2048,512]{1,0:T(8,128)(2,1)} async-done(((bf16[512,512]{1,0:T(8,128)(2,1)}), bf16[2048,512]{1,0:T(8,128)(2,1)}) %all-gather.7.cloned.1.call-update) | async-done | bytes 2097168 | tf_op jit(solution)/shard_map/all_gather | solution.py:47
  58.0 6.1 %fusion.14 = f32[1536,512]{1,0:T(8,128)S(1)} fusion(bf16[1536,2048]{1,0:T(8,128)(2,1)} %param.11, bf16[2048,512]{1,0:T(8,128)(2,1)} %all-gather.7.cloned.1.call-done), kind=kOutput, calls=%fused_computation.26 | convolution fusion | flops 3221225472 | bytes 11534336 | tf_op jit(solution)/shard_map/dot_general | solution.py:50
  64.1 1.9 fusion
  66.0 2.9 add_convert_fusion.1
  68.9 0.0 reduce-scatter.5.cloned.1.call-start
  69.0 35.1 %all-gather.11.cloned.1.call-done = bf16[2048,512]{1,0:T(8,128)(2,1)} async-done(((bf16[512,512]{1,0:T(8,128)(2,1)}), bf16[2048,512]{1,0:T(8,128)(2,1)}) %all-gather.11.cloned.1.call-update) | async-done | bytes 2097168 | tf_op jit(solution)/shard_map/all_gather | solution.py:48
  104.0 6.1 %fusion.15 = f32[1536,512]{1,0:T(8,128)S(1)} fusion(bf16[1536,2048]{1,0:T(8,128)(2,1)} %param.11, bf16[2048,512]{1,0:T(8,128)(2,1)} %all-gather.11.cloned.1.call-done), kind=kOutput, calls=%fused_computation.27 | convolution fusion | flops 3221225472 | bytes 11534336 | tf_op jit(solution)/shard_map/dot_general | solution.py:51
  110.2 1.9 fusion.1
  112.1 2.9 add_convert_fusion
  115.0 18.0 %reduce-scatter.3.cloned.1.call-done = bf16[128,1024]{1,0:T(8,128)(2,1)} async-done(((bf16[512,1024]{1,0:T(8,128)(2,1)}), bf16[128,1024]{1,0:T(8,128)(2,1)}) %reduce-scatter.3.cloned.1.call-update) | async-done | bytes 262160 | tf_op jit(solution)/shard_map/reduce_scatter | solution.py:55
  133.0 28.6 %reduce-scatter.5.cloned.1.call-done = bf16[128,1024]{1,0:T(8,128)(2,1)} async-done(((bf16[512,1024]{1,0:T(8,128)(2,1)}), bf16[128,1024]{1,0:T(8,128)(2,1)}) %reduce-scatter.5.cloned.1.call-update) | async-done | bytes 262160 | tf_op jit(solution)/shard_map/reduce_scatter | solution.py:58
  161.7 46.7 %all-reduce.4.cloned.1.call-done = (bf16[128,1024]{1,0:T(8,128)(2,1)}, bf16[128,1024]{1,0:T(8,128)(2,1)}) async-done(((bf16[128,1024]{1,0:T(8,128)(2,1)}, bf16[128,1024]{1,0:T(8,128)(2,1)}), (bf16[128,1024]{1,0:T(8,128)(2,1)}, bf16[128,1024]{1,0:T(8,128)(2,1)})) %all-reduce.4.cloned.1.call-update) | async-done | bytes 524304 | tf_op jit(solution)/shard_map/psum | solution.py:63
  208.4 3.2 multiply_reduce_fusion.1
  211.6 0.0 all-gather.13.cloned.1.call-start
  211.6 1.9 multiply_reduce_fusion
  213.6 0.0 all-gather.15.cloned.1.call-start
  213.6 0.1 copy-done.5
  213.7 1.8 copy.19
  215.5 17.6 %all-reduce = (f32[]{:T(128)}, f32[]{:T(128)}) all-reduce(f32[]{:T(128)} %get-tuple-element.24, f32[]{:T(128)} %get-tuple-element.20), channel_id=1, replica_groups=mesh['fs'=4,'rep'=4,'tp'=2] {'fs','tp'}, use_global_device_ids=true, to_apply=%region_3.0 | all-reduce | flops 2 | bytes 16 | tf_op jit(solution)/shard_map/psum | solution.py:68
  233.8 23.8 %all-gather.9.cloned.1.call-done = f32[512,1024]{1,0:T(8,128)} async-done(((f32[128,1024]{1,0:T(8,128)}), f32[512,1024]{1,0:T(8,128)}) %all-gather.9.cloned.1.call-update) | async-done | bytes 2097168 | tf_op jit(solution)/shard_map/all_gather | solution.py:75
  257.6 6.7 %subtract_convert_fusion.3 = (bf16[512,1024]{0,1:T(8,128)(2,1)}, f32[512,1024]{0,1:T(8,128)S(1)}) fusion(f32[512,1024]{0,1:T(8,128)} %copy.19, f32[]{:T(128)S(6)} %sqrt.13, f32[512,1024]{1,0:T(8,128)} %all-gather.9.cloned.1.call-done, bf16[512,512]{1,0:T(8,128)(2,1)S(1)} %copy-done.3), kind=kOutput, calls=%fused_computation.3 | convolution fusion | flops 3223322624 | bytes 7864324 | tf_op jit(solution)/shard_map/dot_general | solution.py:78
  264.4 3.0 copy.20
  268.1 36.1 %all-gather.13.cloned.1.call-done = f32[512,1024]{1,0:T(8,128)} async-done(((f32[128,1024]{1,0:T(8,128)}), f32[512,1024]{1,0:T(8,128)}) %all-gather.13.cloned.1.call-update) | async-done | bytes 2097168 | tf_op jit(solution)/shard_map/all_gather | solution.py:76
  304.2 7.5 %subtract_convert_fusion.2 = (bf16[512,1024]{0,1:T(8,128)(2,1)}, f32[512,1024]{0,1:T(8,128)}) fusion(f32[512,1024]{0,1:T(8,128)} %copy.20, f32[]{:T(128)S(6)} %sqrt.15, f32[512,1024]{1,0:T(8,128)} %all-gather.13.cloned.1.call-done, bf16[512,512]{1,0:T(8,128)(2,1)S(1)} %copy-done.4), kind=kOutput, calls=%fused_computation.2 | convolution fusion | flops 3223322624 | bytes 7864324 | tf_op jit(solution)/shard_map/dot_general | solution.py:79
  311.7 1.8 copy.21
  313.5 3.0 copy.22
  316.5 69.5 %all-gather.15.cloned.1.call-done = bf16[2048,1024]{0,1:T(8,128)(2,1)} async-done(((bf16[512,1024]{0,1:T(8,128)(2,1)}), bf16[2048,1024]{0,1:T(8,128)(2,1)}) %all-gather.15.cloned.1.call-update) | async-done | bytes 4194320 | tf_op jit(solution)/shard_map/all_gather | solution.py:85
  385.9 6.4 %copy.23 = bf16[2048,1024]{1,0:T(8,128)(2,1)} copy(bf16[2048,1024]{0,1:T(8,128)(2,1)} %all-gather.15.cloned.1.call-done) | data formatting | bytes 8388608
  392.3 74.4 %all-gather.17.cloned.1.call-done = bf16[2048,1024]{0,1:T(8,128)(2,1)} async-done(((bf16[512,1024]{0,1:T(8,128)(2,1)}), bf16[2048,1024]{0,1:T(8,128)(2,1)}) %all-gather.17.cloned.1.call-update) | async-done | bytes 4194320 | tf_op jit(solution)/shard_map/all_gather | solution.py:86
  466.8 6.5 %copy.24 = bf16[2048,1024]{1,0:T(8,128)(2,1)} copy(bf16[2048,1024]{0,1:T(8,128)(2,1)} %all-gather.17.cloned.1.call-done) | data formatting | bytes 8388608
  (30 shorter events, 0.4 us)
Async XLA Ops:
  7.2 56.9 %copy-start = (bf16[1536,1024]{1,0:T(8,128)(2,1)S(1)}, bf16[1536,1024]{1,0:T(8,128)(2,1)}, u32[]{:S(2)}) copy-start(bf16[1536,1024]{1,0:T(8,128)(2,1)} %param.12) | copy-start | bytes 9437188
  7.2 50.8 %all-gather.7.cloned.1.call-start = ((), (), s32[]{:S(2)}) async-start(), calls=%async_computation.2 | async-start | bytes 2621440 | tf_op jit(solution)/shard_map/all_gather | solution.py:47
  7.9 96.1 %all-gather.11.cloned.1.call-start = ((), (), s32[]{:S(2)}) async-start(), calls=%async_computation.5 | async-start | bytes 2621440 | tf_op jit(solution)/shard_map/all_gather | solution.py:48
  8.7 124.4 %reduce-scatter.3.cloned.1.call-start = ((), (), s32[]{:S(2)}) async-start(), calls=%async_computation.3 | async-start | bytes 1310720 | tf_op jit(solution)/shard_map/reduce_scatter | solution.py:55
  68.9 41.3 %copy-start.2 = (bf16[1536,1024]{1,0:T(8,128)(2,1)S(1)}, bf16[1536,1024]{1,0:T(8,128)(2,1)}, u32[]{:S(2)}) copy-start(bf16[1536,1024]{1,0:T(8,128)(2,1)} %param.13) | copy-start | bytes 9437188
  68.9 92.7 %reduce-scatter.5.cloned.1.call-start = ((), (), s32[]{:S(2)}) async-start(), calls=%async_computation.6 | async-start | bytes 1310720 | tf_op jit(solution)/shard_map/reduce_scatter | solution.py:58
  115.0 96.7 %copy-start.6 = (f32[128,1024]{1,0:T(8,128)S(1)}, f32[128,1024]{1,0:T(8,128)}, u32[]{:S(2)}) copy-start(f32[128,1024]{1,0:T(8,128)} %param.19) | copy-start | bytes 1572868
  115.0 96.6 %copy-start.7 = (f32[128,1024]{1,0:T(8,128)S(1)}, f32[128,1024]{1,0:T(8,128)}, u32[]{:S(2)}) copy-start(f32[128,1024]{1,0:T(8,128)} %param.17) | copy-start | bytes 1572868
  115.0 93.4 %all-reduce.4.cloned.1.call-start = ((), (), s32[]{:S(2)}) async-start(), calls=%async_computation.10 | async-start | bytes 1048576 | tf_op jit(solution)/shard_map/psum | solution.py:63
  161.6 96.0 %all-gather.9.cloned.1.call-start = ((), (), s32[]{:S(2)}) async-start(), calls=%async_computation.4 | async-start | bytes 2621440 | tf_op jit(solution)/shard_map/all_gather | solution.py:75
  208.4 3.3 copy-start.8
  211.5 2.2 copy-start.5
  211.6 92.6 %all-gather.13.cloned.1.call-start = ((), (), s32[]{:S(2)}) async-start(), calls=%async_computation.7 | async-start | bytes 2621440 | tf_op jit(solution)/shard_map/all_gather | solution.py:76
  213.6 44.1 %copy-start.3 = (bf16[512,512]{1,0:T(8,128)(2,1)S(1)}, bf16[512,512]{1,0:T(8,128)(2,1)}, u32[]{:S(2)}) copy-start(bf16[512,512]{1,0:T(8,128)(2,1)} %param.14) | copy-start | bytes 1572868
  213.6 172.4 %all-gather.15.cloned.1.call-start = ((), (), s32[]{:S(2)}) async-start(), calls=%async_computation.8 | async-start | bytes 5242880 | tf_op jit(solution)/shard_map/all_gather | solution.py:85
  264.3 39.9 %copy-start.4 = (bf16[512,512]{1,0:T(8,128)(2,1)S(1)}, bf16[512,512]{1,0:T(8,128)(2,1)}, u32[]{:S(2)}) copy-start(bf16[512,512]{1,0:T(8,128)(2,1)} %param.15) | copy-start | bytes 1572868
  264.3 202.4 %all-gather.17.cloned.1.call-start = ((), (), s32[]{:S(2)}) async-start(), calls=%async_computation.9 | async-start | bytes 5242880 | tf_op jit(solution)/shard_map/all_gather | solution.py:86
  466.8 6.5 %copy-start.1 = (bf16[1536,1024]{1,0:T(8,128)(2,1)S(1)}, bf16[1536,1024]{1,0:T(8,128)(2,1)}, u32[]{:S(2)}) copy-start(bf16[1536,1024]{1,0:T(8,128)(2,1)} %param.12) | copy-start | bytes 9437188
Sparse Core Ops, SparseCore 0:
  9.6 48.3 all-gather.6
  59.5 44.4 all-gather.10
  106.9 26.0 reduce-scatter.2
  135.7 25.7 reduce-scatter.4
  164.4 43.9 all-reduce.3
  211.7 45.8 all-gather.8
  259.8 44.4 all-gather.12
  306.3 79.5 all-gather.14
  387.5 79.2 all-gather.16
where the time goes:
time: 480 us
  waiting for transfers between devices  383 us (80%)
  matrix products  35.9 us (7%)
  local copies, waits for them, and re-layouts  22.7 us (5%)
  blocking collectives  17.6 us (4%)
  between operations  15.3 us (3%)
  other arithmetic  5.05 us (1%)
    all_gather x1, waiting for transfers between devices, body(): lax.all_gather(copy_gate, 'fs', axis=0, tiled=True)  74.4 us
    all_gather x1, waiting for transfers between devices, body(): lax.all_gather(copy_rec, 'fs', axis=0, tiled=True)  69.5 us
    all_gather x1, waiting for transfers between devices, body(): lax.all_gather(factor_rec, 'fs', axis=0, tiled=True)  49.3 us
    psum x1, waiting for transfers between devices, body(): lax.psum(low_rec.astype(jnp.bfloat16), 'rep').astype(jnp.float32)  46.7 us
    all_gather x1, waiting for transfers between devices, body(): lax.all_gather(direc_gate, 'fs', axis=0, tiled=True)  36.1 us
    all_gather x1, waiting for transfers between devices, body(): lax.all_gather(factor_gate, 'fs', axis=0, tiled=True)  35.1 us
    reduce_scatter x1, waiting for transfers between devices, body(): lax.psum_scatter(part_gate.astype(jnp.bfloat16), 'fs', scatter_dimension=...  28.6 us
    all_gather x1, waiting for transfers between devices, body(): lax.all_gather(direc_rec, 'fs', axis=0, tiled=True)  23.8 us
  transfers between devices with their start and end apart: 9, of which 9 were waited for; matrix products, arithmetic and copies ran while one was open for 11% of the time, Pallas kernels for 0%

commit v1 on v0

v1 whole, which is shorter than its diff:
```python
import functools

import jax
import jax.numpy as jnp
from jax import lax
from jax.experimental import pallas as pl
from jax.experimental.pallas import tpu as pltpu
from jax.sharding import PartitionSpec as P

beta_first = 0.8
beta_second = 0.9
scale_floor = 0.25
step_rate = 0.01

MESH = pl.DeviceIdType.MESH
F32 = jnp.float32
BF16 = jnp.bfloat16
TOKEN_TILES = 4


def kernel(
    nf,
    nr,
    x_hbm,
    c0_hbm,
    c1_hbm,
    fac0_hbm,
    fac1_hbm,
    first0,
    first1,
    second0,
    second1,
    fac_out,
    dir_out,
    low_out,
    sum_out,
    x,
    c,
    fac,
    proj,
    part,
    own,
    recv_rep,
    mid,
    recv_fs,
    fst,
    snd,
    low,
    dirs,
    sums,
    sums_in,
    local_sem,
    out_sem,
    fz_s,
    fz_r,
    fr_s,
    fr_r,
    fx_s,
    fx_r,
    pj_s,
    pj_r,
    rr_s,
    rr_r,
    rf_s,
    rf_r,
    dz_s,
    dz_r,
    dr_s,
    dr_r,
    lw_s,
    lw_r,
    sm_s,
    sm_r,
):
    f, r, t = lax.axis_index("fs"), lax.axis_index("rep"), lax.axis_index("tp")
    tokens = x.shape[0]
    rank, cols = dirs.shape[1], dirs.shape[2]
    rows = fac0_hbm.shape[0]
    quarter = rows // nr
    low_rows = rank // nf
    width = cols // nr
    tile = tokens // TOKEN_TILES

    def fpeer(k):
        return lax.rem(f + k, nf)

    def rpeer(k):
        return lax.rem(r + k, nr)

    mine = fac.at[t, pl.ds(pl.multiple_of(f * rows, rows), rows), :]

    @pl.when(t == 0)
    def _():
        pltpu.make_async_copy(fac0_hbm, mine, local_sem.at[0]).start()

    @pl.when(t != 0)
    def _():
        pltpu.make_async_copy(fac1_hbm, mine, local_sem.at[0]).start()

    load_x = pltpu.make_async_copy(x_hbm, x, local_sem.at[1])
    load_x.start()
    loads = [
        pltpu.make_async_copy(c0_hbm, c.at[0], local_sem.at[2]),
        pltpu.make_async_copy(c1_hbm, c.at[1], local_sem.at[3]),
    ]
    lane = pl.ds(pl.multiple_of(r * width, width), width)
    for i, (src, dst) in enumerate(
        ((first0, fst.at[0]), (first1, fst.at[1]), (second0, snd.at[0]), (second1, snd.at[1]))
    ):
        loads.append(pltpu.make_async_copy(src.at[:, lane], dst, local_sem.at[4 + i]))
    for load in loads:
        load.start()

    barrier = pltpu.get_barrier_semaphore()
    for k in range(1, nf):
        pl.semaphore_signal(barrier, inc=1, device_id=(fpeer(k), r, t), device_id_type=MESH)
    for k in range(1, nr):
        pl.semaphore_signal(barrier, inc=1, device_id=(f, rpeer(k), t), device_id_type=MESH)
    pl.semaphore_signal(barrier, inc=1, device_id=(f, r, 1 - t), device_id_type=MESH)
    pl.semaphore_wait(barrier, nf + nr - 1)

    started = []

    def send(src, dst, s_sem, r_sem, device):
        copy = pltpu.make_async_remote_copy(
            src_ref=src, dst_ref=dst, send_sem=s_sem, recv_sem=r_sem,
            device_id=device, device_id_type=MESH,
        )
        copy.start()
        started.append(copy)

    def arrived(ref, s_sem, r_sem, device):
        pltpu.make_async_remote_copy(
            src_ref=ref, dst_ref=ref, send_sem=s_sem, recv_sem=r_sem,
            device_id=device, device_id_type=MESH,
        ).wait_recv()

    sibling = (f, r, 1 - t)

    def fpiece(ff, rr):
        start = pl.multiple_of(ff * rows + rr * quarter, quarter)
        return fac.at[t, pl.ds(start, quarter), :]

    pltpu.make_async_copy(fac0_hbm, mine, local_sem.at[0]).wait()
    for k in range(1, nf):
        send(fpiece(f, r), fpiece(f, r), fz_s.at[k - 1], fz_r.at[k - 1], (fpeer(k), r, t))
    for k in range(1, nf):
        src = fpeer(nf - k)
        arrived(fpiece(src, r), fz_s.at[k - 1], fz_r.at[k - 1], (src, r, t))
        for j in range(1, nr):
            send(fpiece(src, r), fpiece(src, r), fr_s.at[k - 1, j - 1], fr_r.at[k - 1, j - 1], (f, rpeer(j), t))
    for k in range(1, nf):
        src = fpeer(nf - k)
        for j in range(1, nr):
            rsrc = rpeer(nr - j)
            arrived(fpiece(src, rsrc), fr_s.at[k - 1, j - 1], fr_r.at[k - 1, j - 1], (f, rsrc, t))

    load_x.wait()
    for i in range(TOKEN_TILES):
        span = pl.ds(i * tile, tile)
        proj[t, span, :] = jnp.dot(
            x[span, :], fac[t], preferred_element_type=F32
        ).astype(BF16)
        send(proj.at[t, span, :], proj.at[t, span, :], pj_s.at[i], pj_r.at[i], sibling)
    send(fac.at[t], fac.at[t], fx_s, fx_r, sibling)
    for load in loads:
        load.wait()

    def product(p, rr):
        at = pl.ds(pl.multiple_of(rr * width, width), width)
        return lax.dot_general(
            proj[p], c[p, :, at], (((0,), (0,)), ((), ())), preferred_element_type=F32
        )

    order = (t, 1 - t)
    for s, p in enumerate(order):
        if s == 1:
            for i in range(TOKEN_TILES):
                span = pl.ds(i * tile, tile)
                arrived(proj.at[1 - t, span, :], pj_s.at[i], pj_r.at[i], sibling)
        for j in range(1, nr):
            part[s, j - 1] = product(p, rpeer(j)).astype(BF16)
            send(part.at[s, j - 1], recv_rep.at[s, j - 1], rr_s.at[s, j - 1], rr_r.at[s, j - 1], (f, rpeer(j), t))
        own[s] = product(p, r)

    def rank_rows(ff):
        return pl.ds(pl.multiple_of(ff * low_rows, low_rows), low_rows)

    for s in range(2):
        for j in range(1, nr):
            arrived(recv_rep.at[s, j - 1], rr_s.at[s, j - 1], rr_r.at[s, j - 1], (f, rpeer(nr - j), t))
        total = own[s]
        for j in range(1, nr):
            total = total + recv_rep[s, j - 1].astype(F32)
        own[s] = total
        mid[s] = total.astype(BF16)
        for k in range(1, nf):
            send(mid.at[s, rank_rows(fpeer(k)), :], recv_fs.at[s, k - 1], rf_s.at[s, k - 1], rf_r.at[s, k - 1], (fpeer(k), r, t))

    def dpiece(p, ff, rr):
        at = pl.ds(pl.multiple_of(rr * width, width), width)
        return dirs.at[p, rank_rows(ff), at]

    for s, p in enumerate(order):
        for k in range(1, nf):
            arrived(recv_fs.at[s, k - 1], rf_s.at[s, k - 1], rf_r.at[s, k - 1], (fpeer(nf - k), r, t))
        total = own[s, rank_rows(f), :]
        for k in range(1, nf):
            total = total + recv_fs[s, k - 1].astype(F32)
        rounded = total.astype(BF16)
        low[p, :, lane] = rounded
        wide = rounded.astype(F32)
        new_first = beta_first * fst[p] + (1.0 - beta_first) * wide
        new_second = beta_second * snd[p] + (1.0 - beta_second) * wide * wide
        dirs[p, rank_rows(f), lane] = (new_first / jnp.sqrt(new_second)).astype(BF16)
        for k in range(1, nf):
            send(dpiece(p, f, r), dpiece(p, f, r), dz_s.at[s, k - 1], dz_r.at[s, k - 1], (fpeer(k), r, t))
        for j in range(1, nr):
            send(dpiece(p, f, r), dpiece(p, f, r), dr_s.at[s, 0, j - 1], dr_r.at[s, 0, j - 1], (f, rpeer(j), t))
    for s, p in enumerate(order):
        for k in range(1, nf):
            src = fpeer(nf - k)
            arrived(dpiece(p, src, r), dz_s.at[s, k - 1], dz_r.at[s, k - 1], (src, r, t))
            for j in range(1, nr):
                send(dpiece(p, src, r), dpiece(p, src, r), dr_s.at[s, k, j - 1], dr_r.at[s, k, j - 1], (f, rpeer(j), t))
    for j in range(1, nr):
        send(low.at[:, :, lane], low.at[:, :, lane], lw_s.at[j - 1], lw_r.at[j - 1], (f, rpeer(j), t))

    outs = []

    def put(src, dst):
        copy = pltpu.make_async_copy(src, dst, out_sem.at[len(outs)])
        copy.start()
        outs.append(copy)

    arrived(fac.at[1 - t], fx_s, fx_r, sibling)
    put(fac, fac_out)
    for s, p in enumerate(order):
        for k in range(nf):
            src = fpeer(nf - k)
            for j in range(1, nr):
                rsrc = rpeer(nr - j)
                arrived(dpiece(p, src, rsrc), dr_s.at[s, k, j - 1], dr_r.at[s, k, j - 1], (f, rsrc, t))
    put(dirs, dir_out)

    for p in range(2):
        square = dirs[p].astype(F32)
        square = square * square
        sums[p] = jnp.sum(square.reshape(rank // 8, 8, cols), axis=0)
    send(sums, sums_in, sm_s, sm_r, sibling)
    for j in range(1, nr):
        rsrc = rpeer(nr - j)
        at = pl.ds(pl.multiple_of(rsrc * width, width), width)
        arrived(low.at[:, :, at], lw_s.at[j - 1], lw_r.at[j - 1], (f, rsrc, t))
    put(low, low_out)
    arrived(sums_in, sm_s, sm_r, sibling)
    for p in range(2):
        sum_out[p] = sums[p] + sums_in[p]
    for copy in outs:
        copy.wait()
    for copy in started:
        copy.wait_send()


def gather_directions(nf, nr, normed_in, cotans, factors, firsts, seconds):
    tokens, model = normed_in.shape
    cols = cotans[0].shape[1]
    rows, rank = factors[0].shape
    low_rows, width = rank // nf, cols // nr
    dma = pltpu.SemaphoreType.DMA
    anyspec = pl.BlockSpec(memory_space=pl.ANY)
    pair = lambda *shape: [dma(shape), dma(shape)]
    return pl.pallas_call(
        functools.partial(kernel, nf, nr),
        out_shape=(
            jax.ShapeDtypeStruct((2, model, rank), BF16),
            jax.ShapeDtypeStruct((2, rank, cols), BF16),
            jax.ShapeDtypeStruct((2, low_rows, cols), BF16),
            jax.ShapeDtypeStruct((2, 8, cols), F32),
        ),
        in_specs=[anyspec] * 9,
        out_specs=(anyspec, anyspec, anyspec, pl.BlockSpec(memory_space=pltpu.VMEM)),
        scratch_shapes=[
            pltpu.VMEM((tokens, model), BF16),
            pltpu.VMEM((2, tokens, cols), BF16),
            pltpu.VMEM((2, model, rank), BF16),
            pltpu.VMEM((2, tokens, rank), BF16),
            pltpu.VMEM((2, nr - 1, rank, width), BF16),
            pltpu.VMEM((2, rank, width), F32),
            pltpu.VMEM((2, nr - 1, rank, width), BF16),
            pltpu.VMEM((2, rank, width), BF16),
            pltpu.VMEM((2, nf - 1, low_rows, width), BF16),
            pltpu.VMEM((2, low_rows, width), F32),
            pltpu.VMEM((2, low_rows, width), F32),
            pltpu.VMEM((2, low_rows, cols), BF16),
            pltpu.VMEM((2, rank, cols), BF16),
            pltpu.VMEM((2, 8, cols), F32),
            pltpu.VMEM((2, 8, cols), F32),
            dma((8,)),
            dma((3,)),
            *pair(nf - 1),
            *pair(nf - 1, nr - 1),
            dma,
            dma,
            *pair(TOKEN_TILES),
            *pair(2, nr - 1),
            *pair(2, nf - 1),
            *pair(2, nf - 1),
            *pair(2, nf, nr - 1),
            *pair(nr - 1),
            dma,
            dma,
        ],
        cost_estimate=pl.CostEstimate(
            flops=10 * tokens * model * rank, bytes_accessed=400 * 2**20, transcendentals=0
        ),
        compiler_params=pltpu.CompilerParams(
            collective_id=0, has_side_effects=True, vmem_limit_bytes=48 * 2**20
        ),
    )(normed_in, *cotans, *factors, *firsts, *seconds)


def body(
    nf,
    nr,
    nt,
    normed_in,
    cotan_rec,
    cotan_gate,
    factor_rec,
    factor_gate,
    first_rec,
    first_gate,
    second_rec,
    second_gate,
    master_rec,
    master_gate,
):
    r = lax.axis_index("rep")
    factors = (factor_rec, factor_gate)
    firsts = (first_rec, first_gate)
    seconds = (second_rec, second_gate)
    piece = master_rec.shape[0] // nr
    wholes = [
        lax.all_gather(
            lax.dynamic_slice_in_dim(m, r * piece, piece, 0).astype(BF16),
            ("fs", "rep"), axis=0, tiled=True,
        )
        for m in (master_rec, master_gate)
    ]
    fac, dirs, low, sums = gather_directions(
        nf, nr, normed_in, (cotan_rec, cotan_gate), factors, firsts, seconds
    )
    entries = float(dirs.shape[1] * dirs.shape[2] * nt)
    updates, new_firsts, new_seconds, copies = [], [], [], []
    for p in range(2):
        scale = 1.0 / jnp.sqrt(jnp.sum(sums[p]) / entries + scale_floor)
        updates.append(jnp.dot(factors[p], dirs[p], preferred_element_type=F32) * scale)
        wide = low[p].astype(F32)
        new_firsts.append(beta_first * firsts[p] + (1.0 - beta_first) * wide)
        new_seconds.append(beta_second * seconds[p] + (1.0 - beta_second) * wide * wide)
        upd = jnp.dot(fac[p], dirs[p], preferred_element_type=F32) * scale
        copies.append((wholes[p].astype(F32) - step_rate * upd).astype(BF16))
    return (*updates, *new_firsts, *new_seconds, *copies)


def solution(mesh):
    nf, nr, nt = mesh.shape["fs"], mesh.shape["rep"], mesh.shape["tp"]
    return jax.shard_map(
        functools.partial(body, nf, nr, nt),
        mesh=mesh,
        in_specs=(
            P(("fs", "rep"), None),
            P(("fs", "rep"), "tp"),
            P(("fs", "rep"), "tp"),
            P("fs", None),
            P("fs", None),
            P("fs", "tp"),
            P("fs", "tp"),
            P("fs", "tp"),
            P("fs", "tp"),
            P("fs", "tp"),
            P("fs", "tp"),
        ),
        out_specs=(
            P("fs", "tp"),
            P("fs", "tp"),
            P("fs", "tp"),
            P("fs", "tp"),
            P("fs", "tp"),
            P("fs", "tp"),
            P(None, "tp"),
            P(None, "tp"),
        ),
        check_vma=False,
    )
```

time: 480 us -> 208 us (0.43)
  waiting for transfers between devices: 383 us -> 37.9 us
  Pallas kernels: 0 us -> 110 us
  blocking collectives: 17.6 us -> 0 us
  matrix products: 35.9 us -> 22.4 us
    all_gather x6 -> x2, waiting for transfers between devices: 288 us -> 37.9 us  [body(): lax.all_gather(lax.dynamic_slice_in_dim(m, r * piece, piece, 0).astype(BF...]
    pallas_call x0 -> x1, Pallas kernels: none -> 110 us  [gather_directions(): pl.pallas_call(functools.partial(kernel, nf, nr), out_shape=(jax.ShapeDty...]
    psum x1 -> x0, waiting for transfers between devices: 46.7 us -> none  [body(): lax.psum(low_rec.astype(jnp.bfloat16), 'rep').astype(jnp.float32)]
    reduce_scatter x2 -> x0, waiting for transfers between devices: 46.5 us -> none  [the longest x1 28.6 us: body(): lax.psum_scatter(part_gate.astype(jnp.bfloat16), 'fs', scatter_dimension=...]
    psum x1 -> x0, blocking collectives: 17.6 us -> none  [body(): lax.psum((jnp.sum(direc_rec * direc_rec), jnp.sum(direc_gate * direc_gate...]
    dot_general x8 -> x4, matrix products: 35.9 us -> 22.4 us  [the longest x2 15.6 us: body(): upd = jnp.dot(fac[p], dirs[p], preferred_element_type=F32) * scale]
    unnamed x24 -> x26, local copies, waits for them, and re-layouts: 22.7 us -> 15.7 us
  transfers between devices with their start and end apart: 9 -> 2, of which waited for: 9 -> 1; matrix products, arithmetic and copies ran while one was open for 11% -> 12% of each run, Pallas kernels for 0% -> 53%
where the time goes in v1:
time: 208 us; the launch traced here: 207 us
  Pallas kernels  110 us (53%)
  waiting for transfers between devices  37.9 us (18%)
  matrix products  22.4 us (11%)
  local copies, waits for them, and re-layouts  18.2 us (9%)
  between operations  15.5 us (7%)
  other arithmetic  3.46 us (2%)
    pallas_call x1, Pallas kernels, gather_directions(): pl.pallas_call(functools.partial(kernel, nf, nr), out_shape=(jax.ShapeDty...  110 us
    all_gather x2, waiting for transfers between devices, body(): lax.all_gather(lax.dynamic_slice_in_dim(m, r * piece, piece, 0).astype(BF...  37.9 us
    unnamed x26, local copies, waits for them, and re-layouts  15.7 us
    dot_general x2, matrix products, body(): upd = jnp.dot(fac[p], dirs[p], preferred_element_type=F32) * scale  15.6 us
    dot_general x2, matrix products, body(): jnp.dot(factors[p], dirs[p], preferred_element_type=F32) * scale  6.83 us
  transfers between devices with their start and end apart: 2, of which 1 were waited for; matrix products, arithmetic and copies ran while one was open for 12% of the time, Pallas kernels for 53%

profile of v1, /device:TPU:0, one launch (start us, length us, event | category | flops | bytes accessed | tf_op | source)
XLA Modules:
  0.0 207.2 jit_solution(1898273265733177526)
XLA Ops:
  7.2 0.0 copy-start
  7.2 0.0 all-gather.5.cloned.1.call-start
  7.2 1.5 copy-done
  8.8 0.7 dynamic-slice_convert_fusion
  9.5 0.0 all-gather.5.cloned.1.call-update
  9.5 0.0 all-gather.3.cloned.1.call-start
  9.6 1.8 dynamic-slice_convert_fusion.1
  11.4 0.0 all-gather.3.cloned.1.call-update
  11.4 0.0 copy-start.2
  11.4 1.0 copy-done.2
  12.5 0.0 copy-start.4
  12.5 1.0 copy-done.4
  13.5 1.0 copy-done.6
  14.5 1.0 copy-done.7
  15.6 1.0 copy-done.9
  16.6 1.0 copy-done.11
  17.7 109.7 %shard_map.170 = (bf16[2,2048,512]{2,1,0:T(8,128)(2,1)}, bf16[2,512,1024]{2,1,0:T(8,128)(2,1)S(1)}, bf16[2,128,1024]{2,1,0:T(8,128)(2,1)S(1)}, f32[2,8,1024]{2,1,0:T(8,128)S(1)}) custom-call(bf16[1536,2048]{1,0:T(8,128)(2,1)} %x_hbm.1, bf16[1536,1024]{1,0:T(8,128)(2,1)} %c0_hbm.1, bf16[1536,1024]{1,0:T(8,128)(2,1)} %c1_hbm.1, ...), custom_call_target="tpu_custom_call" | custom-call | flops 16106127360 | bytes 419430400 | tf_op jit(solution)/shard_map/pallas_call | solution.py:273
  127.4 0.0 copy-start.1
  127.4 1.3 copy-done.1
  128.7 0.8 copy-done.8
  129.5 0.6 slice_reduce_fusion
  131.5 0.0 copy-done.10
  131.5 3.3 %multiply_bitcast_fusion = f32[512,1024]{0,1:T(8,128)} fusion(bf16[512,512]{1,0:T(8,128)(2,1)S(1)} %copy-done.10, f32[]{:T(128)S(6)} %sqrt.7, bf16[2,512,1024]{2,1,0:T(8,128)(2,1)} %copy-done.1), kind=kOutput, calls=%fused_computation.6 | convolution fusion | flops 537395200 | bytes 3670020 | tf_op jit(solution)/shard_map/dot_general | solution.py:358
  134.8 2.9 %copy.20 = f32[512,1024]{1,0:T(8,128)} copy(f32[512,1024]{0,1:T(8,128)} %multiply_bitcast_fusion) | data formatting | bytes 4194304
  137.7 3.5 %multiply_bitcast_fusion.1 = f32[512,1024]{0,1:T(8,128)} fusion(bf16[512,512]{1,0:T(8,128)(2,1)} %fac0_hbm.1, f32[]{:T(128)S(6)} %sqrt.6, bf16[2,512,1024]{2,1,0:T(8,128)(2,1)} %copy-done.1), kind=kOutput, calls=%fused_computation.7 | convolution fusion | flops 537395200 | bytes 3670020 | tf_op jit(solution)/shard_map/dot_general | solution.py:358
  141.2 2.9 %copy.19 = f32[512,1024]{1,0:T(8,128)} copy(f32[512,1024]{0,1:T(8,128)} %multiply_bitcast_fusion.1) | data formatting | bytes 4194304
  144.1 0.0 copy-done.3
  144.1 0.0 copy-done.5
  144.1 2.9 %fusion.15 = (f32[128,1024]{1,0:T(8,128)}, f32[128,1024]{1,0:T(8,128)}, f32[128,1024]{1,0:T(8,128)}, f32[128,1024]{1,0:T(8,128)}) fusion(f32[128,1024]{1,0:T(8,128)} %second1.1, bf16[2,128,1024]{2,1,0:T(8,128)(2,1)} %copy-done.8, f32[128,1024]{1,0:T(8,128)} %second0.1, f32[128,1024]{1,0:T(8,128)S(1)} %copy-done.5, f32[128,1024]{1,0:T(8,128)S(1)} %copy-done.3), kind=kLoop, calls=%fused_computation.25 | loop fusion | flops 2097152 | bytes 4718592 | tf_op jit(solution)/shard_map/add | solution.py:361
  147.0 7.8 %subtract_convert_fusion = bf16[2048,1024]{1,0:T(8,128)(2,1)} fusion(bf16[2048,1024]{1,0:T(8,128)(2,1)} %all-gather.5.cloned.1.call-done, f32[]{:T(128)S(6)} %sqrt.7, bf16[2,2048,512]{2,1,0:T(8,128)(2,1)} %get-tuple-element.15, bf16[2,512,1024]{2,1,0:T(8,128)(2,1)} %copy-done.1), kind=kOutput, calls=%fused_computation | convolution fusion | flops 2157969408 | bytes 11534340 | tf_op jit(solution)/shard_map/dot_general | solution.py:362
  154.8 37.9 %all-gather.3.cloned.1.call-done = bf16[2048,1024]{1,0:T(8,128)(2,1)} async-done(((bf16[128,1024]{1,0:T(8,128)(2,1)}), bf16[2048,1024]{1,0:T(8,128)(2,1)}) %all-gather.3.cloned.1.call-update) | async-done | bytes 4194320 | tf_op jit(solution)/shard_map/all_gather | solution.py:345
  192.6 7.8 %subtract_convert_fusion.1 = bf16[2048,1024]{1,0:T(8,128)(2,1)} fusion(bf16[2048,1024]{1,0:T(8,128)(2,1)} %all-gather.3.cloned.1.call-done, f32[]{:T(128)S(6)} %sqrt.6, bf16[2,2048,512]{2,1,0:T(8,128)(2,1)} %get-tuple-element.15, bf16[2,512,1024]{2,1,0:T(8,128)(2,1)} %copy-done.1), kind=kOutput, calls=%fused_computation.1 | convolution fusion | flops 2157969408 | bytes 11534340 | tf_op jit(solution)/shard_map/dot_general | solution.py:362
  (9 shorter events, 0.0 us)
Async XLA Ops:
  7.2 1.6 copy-start
  7.2 139.8 %all-gather.5.cloned.1.call-start = ((), (), s32[]{:S(2)}) async-start(), calls=%async_computation.1 | async-start | bytes 4456448 | tf_op jit(solution)/shard_map/all_gather | solution.py:345
  9.5 183.1 %all-gather.3.cloned.1.call-start = ((), (), s32[]{:S(2)}) async-start(), calls=%async_computation | async-start | bytes 4456448 | tf_op jit(solution)/shard_map/all_gather | solution.py:345
  11.4 1.0 copy-start.2
  12.5 1.0 copy-start.4
  13.5 1.0 copy-start.6
  14.5 1.0 copy-start.7
  15.6 1.0 copy-start.9
  16.6 1.0 copy-start.11
  17.7 113.8 %copy-start.10 = (bf16[512,512]{1,0:T(8,128)(2,1)S(1)}, bf16[512,512]{1,0:T(8,128)(2,1)}, u32[]{:S(2)}) copy-start(bf16[512,512]{1,0:T(8,128)(2,1)} %fac1_hbm.1) | copy-start | bytes 1572868
  127.4 1.3 copy-start.1
  128.7 0.8 copy-start.8
  137.7 6.4 %copy-start.3 = (f32[128,1024]{1,0:T(8,128)S(1)}, f32[128,1024]{1,0:T(8,128)}, u32[]{:S(2)}) copy-start(f32[128,1024]{1,0:T(8,128)} %first0.1) | copy-start | bytes 1572868
  137.7 6.4 %copy-start.5 = (f32[128,1024]{1,0:T(8,128)S(1)}, f32[128,1024]{1,0:T(8,128)}, u32[]{:S(2)}) copy-start(f32[128,1024]{1,0:T(8,128)} %first1.1) | copy-start | bytes 1572868
Sparse Core Ops, SparseCore 0:
  10.8 105.6 all-gather.4
  119.2 73.3 all-gather.2

commit v2 on v1

--- a/solution.py
+++ b/solution.py
@@ -30,9 +30,11 @@
     first1,
     second0,
     second1,
+    mast_hbm,
     fac_out,
     dir_out,
     low_out,
+    mast_out,
     sum_out,
     x,
     c,
@@ -49,6 +51,7 @@
     dirs,
     sums,
     sums_in,
+    mast,
     local_sem,
     out_sem,
     fz_s,
@@ -71,6 +74,10 @@
     lw_r,
     sm_s,
     sm_r,
+    mz_s,
+    mz_r,
+    mr_s,
+    mr_r,
 ):
     f, r, t = lax.axis_index("fs"), lax.axis_index("rep"), lax.axis_index("tp")
     tokens = x.shape[0]
@@ -97,6 +104,10 @@
     def _():
         pltpu.make_async_copy(fac1_hbm, mine, local_sem.at[0]).start()
 
+    load_m = pltpu.make_async_copy(
+        mast_hbm, mast.at[pl.ds(pl.multiple_of(f * rows, rows), rows), :], local_sem.at[8]
+    )
+    load_m.start()
     load_x = pltpu.make_async_copy(x_hbm, x, local_sem.at[1])
     load_x.start()
     loads = [
@@ -144,6 +155,21 @@
     pltpu.make_async_copy(fac0_hbm, mine, local_sem.at[0]).wait()
     for k in range(1, nf):
         send(fpiece(f, r), fpiece(f, r), fz_s.at[k - 1], fz_r.at[k - 1], (fpeer(k), r, t))
+
+    def mpiece(ff, rr):
+        start = pl.multiple_of(ff * rows + rr * quarter, quarter)
+        return mast.at[pl.ds(start, quarter), :]
+
+    def pass_master(k):
+        src = fpeer(nf - k)
+        arrived(mpiece(src, r), mz_s.at[k - 1], mz_r.at[k - 1], (src, r, t))
+        for j in range(1, nr):
+            send(mpiece(src, r), mpiece(src, r), mr_s.at[k - 1, j - 1], mr_r.at[k - 1, j - 1], (f, rpeer(j), t))
+
+    third = (nf - 1) // 3
+    load_m.wait()
+    for k in range(1, nf):
+        send(mpiece(f, r), mpiece(f, r), mz_s.at[k - 1], mz_r.at[k - 1], (fpeer(k), r, t))
     for k in range(1, nf):
         src = fpeer(nf - k)
         arrived(fpiece(src, r), fz_s.at[k - 1], fz_r.at[k - 1], (src, r, t))
@@ -154,6 +180,9 @@
         for j in range(1, nr):
             rsrc = rpeer(nr - j)
             arrived(fpiece(src, rsrc), fr_s.at[k - 1, j - 1], fr_r.at[k - 1, j - 1], (f, rsrc, t))
+
+    for k in range(1, 1 + third):
+        pass_master(k)
 
     load_x.wait()
     for i in range(TOKEN_TILES):
@@ -182,6 +211,9 @@
             part[s, j - 1] = product(p, rpeer(j)).astype(BF16)
             send(part.at[s, j - 1], recv_rep.at[s, j - 1], rr_s.at[s, j - 1], rr_r.at[s, j - 1], (f, rpeer(j), t))
         own[s] = product(p, r)
+
+    for k in range(1 + third, 1 + 2 * third):
+        pass_master(k)
 
     def rank_rows(ff):
         return pl.ds(pl.multiple_of(ff * low_rows, low_rows), low_rows)
@@ -217,6 +249,8 @@
             send(dpiece(p, f, r), dpiece(p, f, r), dz_s.at[s, k - 1], dz_r.at[s, k - 1], (fpeer(k), r, t))
         for j in range(1, nr):
             send(dpiece(p, f, r), dpiece(p, f, r), dr_s.at[s, 0, j - 1], dr_r.at[s, 0, j - 1], (f, rpeer(j), t))
+    for k in range(1 + 2 * third, nf):
+        pass_master(k)
     for s, p in enumerate(order):
         for k in range(1, nf):
             src = fpeer(nf - k)
@@ -253,6 +287,12 @@
         at = pl.ds(pl.multiple_of(rsrc * width, width), width)
         arrived(low.at[:, :, at], lw_s.at[j - 1], lw_r.at[j - 1], (f, rsrc, t))
     put(low, low_out)
+    for k in range(1, nf):
+        src = fpeer(nf - k)
+        for j in range(1, nr):
+            rsrc = rpeer(nr - j)
+            arrived(mpiece(src, rsrc), mr_s.at[k - 1, j - 1], mr_r.at[k - 1, j - 1], (f, rsrc, t))
+    put(mast, mast_out)
     arrived(sums_in, sm_s, sm_r, sibling)
     for p in range(2):
         sum_out[p] = sums[p] + sums_in[p]
@@ -262,7 +302,7 @@
         copy.wait_send()
 
 
-def gather_directions(nf, nr, normed_in, cotans, factors, firsts, seconds):
+def gather_directions(nf, nr, normed_in, cotans, factors, firsts, seconds, master):
     tokens, model = normed_in.shape
     cols = cotans[0].shape[1]
     rows, rank = factors[0].shape
@@ -276,10 +316,11 @@
             jax.ShapeDtypeStruct((2, model, rank), BF16),
             jax.ShapeDtypeStruct((2, rank, cols), BF16),
             jax.ShapeDtypeStruct((2, low_rows, cols), BF16),
+            jax.ShapeDtypeStruct((model, master.shape[1]), BF16),
             jax.ShapeDtypeStruct((2, 8, cols), F32),
         ),
-        in_specs=[anyspec] * 9,
-        out_specs=(anyspec, anyspec, anyspec, pl.BlockSpec(memory_space=pltpu.VMEM)),
+        in_specs=[anyspec] * 10,
+        out_specs=(anyspec, anyspec, anyspec, anyspec, pl.BlockSpec(memory_space=pltpu.VMEM)),
         scratch_shapes=[
             pltpu.VMEM((tokens, model), BF16),
             pltpu.VMEM((2, tokens, cols), BF16),
@@ -296,8 +337,9 @@
             pltpu.VMEM((2, rank, cols), BF16),
             pltpu.VMEM((2, 8, cols), F32),
             pltpu.VMEM((2, 8, cols), F32),
-            dma((8,)),
-            dma((3,)),
+            pltpu.VMEM((model, master.shape[1]), BF16),
+            dma((9,)),
+            dma((4,)),
             *pair(nf - 1),
             *pair(nf - 1, nr - 1),
             dma,
@@ -310,14 +352,16 @@
             *pair(nr - 1),
             dma,
             dma,
+            *pair(nf - 1),
+            *pair(nf - 1, nr - 1),
         ],
         cost_estimate=pl.CostEstimate(
             flops=10 * tokens * model * rank, bytes_accessed=400 * 2**20, transcendentals=0
         ),
         compiler_params=pltpu.CompilerParams(
-            collective_id=0, has_side_effects=True, vmem_limit_bytes=48 * 2**20
+            collective_id=0, has_side_effects=True, vmem_limit_bytes=60 * 2**20
         ),
-    )(normed_in, *cotans, *factors, *firsts, *seconds)
+    )(normed_in, *cotans, *factors, *firsts, *seconds, master)
 
 
 def body(
@@ -341,16 +385,19 @@
     firsts = (first_rec, first_gate)
     seconds = (second_rec, second_gate)
     piece = master_rec.shape[0] // nr
-    wholes = [
-        lax.all_gather(
-            lax.dynamic_slice_in_dim(m, r * piece, piece, 0).astype(BF16),
-            ("fs", "rep"), axis=0, tiled=True,
-        )
-        for m in (master_rec, master_gate)
-    ]
-    fac, dirs, low, sums = gather_directions(
-        nf, nr, normed_in, (cotan_rec, cotan_gate), factors, firsts, seconds
+    half = 3 * master_gate.shape[1] // 4
+
+    def gathered(m):
+        own = lax.dynamic_slice_in_dim(m, r * piece, piece, 0).astype(BF16)
+        return lax.all_gather(own, ("fs", "rep"), axis=0, tiled=True)
+
+    whole_rec = gathered(master_rec)
+    gate_right = gathered(master_gate[:, half:])
+    fac, dirs, low, gate_left, sums = gather_directions(
+        nf, nr, normed_in, (cotan_rec, cotan_gate), factors, firsts, seconds,
+        master_gate[:, :half].astype(BF16),
     )
+    wholes = (whole_rec, jnp.concatenate((gate_left, gate_right), axis=1))
     entries = float(dirs.shape[1] * dirs.shape[2] * nt)
     updates, new_firsts, new_seconds, copies = [], [], [], []
     for p in range(2):

time: 208 us -> 188 us (0.904)
  waiting for transfers between devices: 37.9 us -> 10.8 us
  Pallas kernels: 110 us -> 124 us
  local copies, waits for them, and re-layouts: 18.2 us -> 10.7 us
    all_gather x2, waiting for transfers between devices: 37.9 us -> 10.8 us  [gathered(): return lax.all_gather(own, ('fs', 'rep'), axis=0, tiled=True)]
    pallas_call x1, Pallas kernels: 110 us -> 124 us  [gather_directions(): pl.pallas_call(functools.partial(kernel, nf, nr), out_shape=(jax.ShapeDty...]
    unnamed x26 -> x10, local copies, waits for them, and re-layouts: 15.7 us -> 5.78 us
    slice x0 -> x2, local copies, waits for them, and re-layouts: none -> 3.58 us  [the longest x1 2.37 us: body(): master_gate[:, :half].astype(BF16)]
  transfers between devices with their start and end apart: 2 -> 2, of which waited for: 1 -> 1; matrix products, arithmetic and copies ran while one was open for 12% -> 15% of each run, Pallas kernels for 53% -> 66%
where the time goes in v2:
time: 188 us
  Pallas kernels  124 us (66%)
  matrix products  22.4 us (12%)
  between operations  15.5 us (8%)
  waiting for transfers between devices  10.8 us (6%)
  local copies, waits for them, and re-layouts  10.7 us (6%)
  other arithmetic  4.26 us (2%)
    pallas_call x1, Pallas kernels, gather_directions(): pl.pallas_call(functools.partial(kernel, nf, nr), out_shape=(jax.ShapeDty...  124 us
    dot_general x2, matrix products, body(): upd = jnp.dot(fac[p], dirs[p], preferred_element_type=F32) * scale  15.6 us
    all_gather x2, waiting for transfers between devices, gathered(): return lax.all_gather(own, ('fs', 'rep'), axis=0, tiled=True)  10.8 us
    dot_general x2, matrix products, body(): jnp.dot(factors[p], dirs[p], preferred_element_type=F32) * scale  6.83 us
    unnamed x10, local copies, waits for them, and re-layouts  5.78 us
  transfers between devices with their start and end apart: 2, of which 1 were waited for; matrix products, arithmetic and copies ran while one was open for 15% of the time, Pallas kernels for 66%

profile of v2, /device:TPU:0, one launch (start us, length us, event | category | flops | bytes accessed | tf_op | source)
XLA Modules:
  0.0 187.9 jit_solution(4987716220655002658)
XLA Ops:
  7.2 0.0 copy-start
  7.2 0.0 all-gather.5.cloned.1.call-start
  7.2 1.2 slice.41
  8.4 0.6 dynamic-slice_convert_fusion.1
  9.1 0.0 all-gather.5.cloned.1.call-update
  9.1 0.0 all-gather.3.cloned.1.call-start
  9.2 0.0 copy-done
  9.2 0.7 dynamic-slice_convert_fusion
  9.9 0.0 all-gather.3.cloned.1.call-update
  9.9 2.4 %slice.75.mast_hbm = bf16[512,768]{1,0:T(8,128)(2,1)} slice(f32[512,1024]{1,0:T(8,128)} %param.21), slice={[0:512], [0:768]} | slice | bytes 1572864 | tf_op jit(solution)/shard_map/slice | solution.py:398
  12.3 0.0 copy-start.3
  12.3 124.1 %shard_map.170 = (bf16[2,2048,512]{2,1,0:T(8,128)(2,1)}, bf16[2,512,1024]{2,1,0:T(8,128)(2,1)}, bf16[2,128,1024]{2,1,0:T(8,128)(2,1)}, bf16[2048,768]{1,0:T(8,128)(2,1)}, f32[2,8,1024]{2,1,0:T(8,128)}) custom-call(bf16[1536,2048]{1,0:T(8,128)(2,1)} %x_hbm.1, bf16[1536,1024]{1,0:T(8,128)(2,1)} %c0_hbm.1, bf16[1536,1024]{1,0:T(8,128)(2,1)} %c1_hbm.1, ...), custom_call_target="tpu_custom_call" | custom-call | flops 16106127360 | bytes 419430400 | tf_op jit(solution)/shard_map/pallas_call | solution.py:313
  136.4 1.4 slice_reduce_fusion
  139.2 0.0 copy-done.3
  139.2 3.3 %multiply_bitcast_fusion = f32[512,1024]{0,1:T(8,128)} fusion(bf16[512,512]{1,0:T(8,128)(2,1)S(1)} %copy-done.3, f32[]{:T(128)S(6)} %sqrt.7, bf16[2,512,1024]{2,1,0:T(8,128)(2,1)} %get-tuple-element.13), kind=kOutput, calls=%fused_computation.6 | convolution fusion | flops 537395200 | bytes 3670020 | tf_op jit(solution)/shard_map/dot_general | solution.py:405
  142.5 2.9 %copy.20 = f32[512,1024]{1,0:T(8,128)} copy(f32[512,1024]{0,1:T(8,128)} %multiply_bitcast_fusion) | data formatting | bytes 4194304
  145.4 0.0 copy-start.1
  145.4 0.0 copy-start.2
  145.4 3.5 %multiply_bitcast_fusion.1 = f32[512,1024]{0,1:T(8,128)} fusion(bf16[512,512]{1,0:T(8,128)(2,1)} %fac0_hbm.1, f32[]{:T(128)S(6)} %sqrt.6, bf16[2,512,1024]{2,1,0:T(8,128)(2,1)} %get-tuple-element.13), kind=kOutput, calls=%fused_computation.7 | convolution fusion | flops 537395200 | bytes 3670020 | tf_op jit(solution)/shard_map/dot_general | solution.py:405
  148.9 2.9 %copy.19 = f32[512,1024]{1,0:T(8,128)} copy(f32[512,1024]{0,1:T(8,128)} %multiply_bitcast_fusion.1) | data formatting | bytes 4194304
  151.8 0.0 copy-done.1
  151.8 0.0 copy-done.2
  151.8 2.9 %fusion.15 = (f32[128,1024]{1,0:T(8,128)}, f32[128,1024]{1,0:T(8,128)}, f32[128,1024]{1,0:T(8,128)}, f32[128,1024]{1,0:T(8,128)}) fusion(f32[128,1024]{1,0:T(8,128)} %second1.1, bf16[2,128,1024]{2,1,0:T(8,128)(2,1)} %get-tuple-element.15, f32[128,1024]{1,0:T(8,128)} %second0.1, f32[128,1024]{1,0:T(8,128)S(1)} %copy-done.2, f32[128,1024]{1,0:T(8,128)S(1)} %copy-done.1), kind=kLoop, calls=%fused_computation.26 | loop fusion | flops 2097152 | bytes 4718592 | tf_op jit(solution)/shard_map/add | solution.py:408
  154.6 0.0 all-gather.5.cloned.1.call-done
  154.6 7.8 %subtract_convert_fusion = bf16[2048,1024]{1,0:T(8,128)(2,1)} fusion(bf16[2048,256]{1,0:T(8,128)(2,1)} %all-gather.5.cloned.1.call-done, bf16[2048,768]{1,0:T(8,128)(2,1)} %get-tuple-element.17, f32[]{:T(128)S(6)} %sqrt.7, bf16[2,2048,512]{2,1,0:T(8,128)(2,1)} %get-tuple-element.16, bf16[2,512,1024]{2,1,0:T(8,128)(2,1)} %get-tuple-element.13), kind=kOutput, calls=%fused_computation | convolution fusion | flops 2164260864 | bytes 11534340 | tf_op jit(solution)/shard_map/dot_general | solution.py:409
  162.5 10.8 %all-gather.3.cloned.1.call-done = bf16[2048,1024]{1,0:T(8,128)(2,1)} async-done(((bf16[128,1024]{1,0:T(8,128)(2,1)}), bf16[2048,1024]{1,0:T(8,128)(2,1)}) %all-gather.3.cloned.1.call-update) | async-done | bytes 4194320 | tf_op jit(solution)/shard_map/all_gather | solution.py:392
  173.3 7.8 %subtract_convert_fusion.1 = bf16[2048,1024]{1,0:T(8,128)(2,1)} fusion(bf16[2048,1024]{1,0:T(8,128)(2,1)} %all-gather.3.cloned.1.call-done, f32[]{:T(128)S(6)} %sqrt.6, bf16[2,2048,512]{2,1,0:T(8,128)(2,1)} %get-tuple-element.16, bf16[2,512,1024]{2,1,0:T(8,128)(2,1)} %get-tuple-element.13), kind=kOutput, calls=%fused_computation.1 | convolution fusion | flops 2157969408 | bytes 11534340 | tf_op jit(solution)/shard_map/dot_general | solution.py:409
Async XLA Ops:
  7.2 2.0 %copy-start = (f32[512,1024]{1,0:T(8,128)S(1)}, f32[512,1024]{1,0:T(8,128)}, u32[]{:S(2)}) copy-start(f32[512,1024]{1,0:T(8,128)} %param.20) | copy-start | bytes 6291460
  7.2 147.5 %all-gather.5.cloned.1.call-start = ((), (), s32[]{:S(2)}) async-start(), calls=%async_computation.1 | async-start | bytes 1114112 | tf_op jit(solution)/shard_map/all_gather | solution.py:392
  9.1 164.2 %all-gather.3.cloned.1.call-start = ((), (), s32[]{:S(2)}) async-start(), calls=%async_computation | async-start | bytes 4456448 | tf_op jit(solution)/shard_map/all_gather | solution.py:392
  12.3 126.9 %copy-start.3 = (bf16[512,512]{1,0:T(8,128)(2,1)S(1)}, bf16[512,512]{1,0:T(8,128)(2,1)}, u32[]{:S(2)}) copy-start(bf16[512,512]{1,0:T(8,128)(2,1)} %fac1_hbm.1) | copy-start | bytes 1572868
  145.4 6.4 %copy-start.1 = (f32[128,1024]{1,0:T(8,128)S(1)}, f32[128,1024]{1,0:T(8,128)}, u32[]{:S(2)}) copy-start(f32[128,1024]{1,0:T(8,128)} %first0.1) | copy-start | bytes 1572868
  145.4 6.4 %copy-start.2 = (f32[128,1024]{1,0:T(8,128)S(1)}, f32[128,1024]{1,0:T(8,128)}, u32[]{:S(2)}) copy-start(f32[128,1024]{1,0:T(8,128)} %first1.1) | copy-start | bytes 1572868
Sparse Core Ops, SparseCore 0:
  10.7 74.7 all-gather.4
  88.8 84.3 all-gather.2
